TPU v7x, 32 devices: a whole 2x2x4 slice. The times are simulated.
32 devices in a mesh: sp: 8 (over z, y), dp: 4 (over x, core).
Axes of the slice: x: 2, y: 2, z: 4, core: 2. Of those that a mesh axis runs over, the one named last changes fastest.
Arguments:
- query: bfloat16 [4, 1536, 3072], P('dp', 'sp'), may hold values from -18 to 18
- latent: bfloat16 [4, 1536, 1024], P('dp', 'sp'), may hold values from -6 to 6
- rope_key: bfloat16 [4, 1536, 32], P('dp', 'sp'), may hold values from -5 to 5
- latent_norm_gain: float32 [1024], replicated, may hold values from 0.1 to 1.9
- key_up_matrix: bfloat16 [2048, 1024], P('dp'), may hold values from -0.1875 to 0.1875
- value_up_matrix: bfloat16 [2048, 1024], P('dp'), may hold values from -0.1875 to 0.1875
- out_grad: bfloat16 [4, 1536, 2048], P('dp', 'sp'), may hold values from -6 to 6
Outputs:
- query_grad: bfloat16 [4, 1536, 3072], P('dp', 'sp')
- latent_grad: float32 [4, 1536, 1024], P('dp', 'sp')
- rope_key_grad: float32 [4, 1536, 32], P('dp', 'sp')
- key_weight_grad: float32 [2048, 1024], P('dp')
- value_weight_grad: float32 [2048, 1024], P('dp')
- gain_grad: float32 [1024], replicated
All inputs are finite; a program needn't handle non-finite values.
Results may differ from a plain program's by a relative error of at most 0.011.
Values may be sent and summed in bfloat16 or wider, within the bound.
A program may use at most 256 MiB of HBM per device.

v0:
```python
import jax
import jax.numpy as jnp
from jax import lax
from jax.sharding import PartitionSpec as P

ATTENTION_HEADS = 32
PLAIN_HEAD_WIDTH = 64
ROPE = 32
VALUE_HEAD_WIDTH = 64
SPAN = 64
eps = 1e-06
rope_base = 10000.0


def rotate(values, cosine, sine):
    half = values.shape[-1] // 2
    first = values[..., :half]
    second = values[..., half:]
    return jnp.concatenate(
        [first * cosine - second * sine, second * cosine + first * sine], axis=-1
    )


def angles(length, width):
    inverse = 1.0 / rope_base ** (jnp.arange(0, width, 2, dtype=jnp.float32) / width)
    turned = jnp.arange(length, dtype=jnp.float32)[:, None] * inverse[None, :]
    return (jnp.cos(turned), jnp.sin(turned))


def attend_backward(arrived, rope_full):
    f32 = jnp.float32
    bf16 = jnp.bfloat16
    length = arrived.shape[0]
    local_heads = arrived.shape[1]
    width = PLAIN_HEAD_WIDTH + ROPE
    scale = width ** (-0.5)
    block = 512
    cosine, sine = angles(length, ROPE)
    neg = jnp.finfo(f32).min
    q_nope = arrived[:, :, :PLAIN_HEAD_WIDTH]
    q_rope = rotate(
        arrived[:, :, PLAIN_HEAD_WIDTH:width].astype(f32), cosine[:, None, :], sine[:, None, :]
    ).astype(bf16)
    key_nope = arrived[:, :, width : width + PLAIN_HEAD_WIDTH]
    values = arrived[:, :, width + PLAIN_HEAD_WIDTH : width + PLAIN_HEAD_WIDTH + VALUE_HEAD_WIDTH]
    d_out = arrived[:, :, width + PLAIN_HEAD_WIDTH + VALUE_HEAD_WIDTH :]
    k_rope = rotate(rope_full.astype(f32), cosine, sine).astype(bf16)
    dk_nope = jnp.zeros((length, local_heads, PLAIN_HEAD_WIDTH), f32)
    dk_rope = jnp.zeros((length, ROPE), f32)
    d_vals = jnp.zeros((length, local_heads, VALUE_HEAD_WIDTH), f32)
    dq_parts = []
    for begin in range(0, length, block):
        end = begin + block
        qn = q_nope[begin:end]
        qr = q_rope[begin:end]
        go = d_out[begin:end]
        scores = jnp.einsum("qhd,khd->hqk", qn, key_nope[:end], preferred_element_type=f32)
        scores = (
            scores + jnp.einsum("qhd,kd->hqk", qr, k_rope[:end], preferred_element_type=f32)
        ) * scale
        q_seg = jnp.arange(begin, end) // SPAN
        k_seg = jnp.arange(end) // SPAN
        allowed = k_seg[None, :] <= q_seg[:, None]
        scores = jnp.where(allowed[None], scores, neg)
        probs = jax.nn.softmax(scores, axis=-1)
        d_probs = jnp.einsum("qhd,khd->hqk", go, values[:end], preferred_element_type=f32)
        d_scores = probs * (d_probs - jnp.sum(probs * d_probs, axis=-1, keepdims=True))
        ds_b = d_scores.astype(bf16)
        p_b = probs.astype(bf16)
        dq_n = jnp.einsum("hqk,khd->qhd", ds_b, key_nope[:end], preferred_element_type=f32) * scale
        dq_r = jnp.einsum("hqk,kd->qhd", ds_b, k_rope[:end], preferred_element_type=f32) * scale
        dq_r = rotate(dq_r, cosine[begin:end, None, :], -sine[begin:end, None, :])
        dq_parts.append(jnp.concatenate([dq_n, dq_r], axis=-1).astype(bf16))
        dk_nope = dk_nope.at[:end].add(
            jnp.einsum("hqk,qhd->khd", ds_b, qn, preferred_element_type=f32) * scale
        )
        dk_rope = dk_rope.at[:end].add(
            jnp.einsum("hqk,qhd->kd", ds_b, qr, preferred_element_type=f32) * scale
        )
        d_vals = d_vals.at[:end].add(
            jnp.einsum("hqk,qhd->khd", p_b, go, preferred_element_type=f32)
        )
    query_part = jnp.concatenate(dq_parts, axis=0)
    grads = jnp.concatenate([query_part, dk_nope.astype(bf16), d_vals.astype(bf16)], axis=-1)
    return (grads, rotate(dk_rope, cosine, -sine))


def local(query, latent, rope_key, latent_norm_gain, key_up_matrix, value_up_matrix, out_grad):
    f32 = jnp.float32
    bf16 = jnp.bfloat16
    tokens = latent.shape[1]
    width = PLAIN_HEAD_WIDTH + ROPE
    head_cols = ATTENTION_HEADS * PLAIN_HEAD_WIDTH
    lat = latent[0].astype(f32)
    inv_rms = lax.rsqrt(jnp.mean(lat * lat, axis=-1, keepdims=True) + eps)
    normed = lat * inv_rms
    nlat = (normed * latent_norm_gain).astype(bf16)
    stacked = jnp.stack([key_up_matrix, value_up_matrix])
    whole = lax.all_gather(stacked, "dp", axis=1, tiled=True)
    kv_tok = jnp.einsum("tc,gnc->tgn", nlat, whole, preferred_element_type=f32).astype(bf16)
    heads_query = query[0].reshape(tokens, ATTENTION_HEADS, width)
    key_nope = kv_tok[:, 0].reshape(tokens, ATTENTION_HEADS, PLAIN_HEAD_WIDTH)
    values = kv_tok[:, 1].reshape(tokens, ATTENTION_HEADS, VALUE_HEAD_WIDTH)
    d_out = out_grad[0].reshape(tokens, ATTENTION_HEADS, VALUE_HEAD_WIDTH)
    packed = jnp.concatenate([heads_query, key_nope, values, d_out], axis=2)
    arrived = lax.all_to_all(packed, "sp", split_axis=1, concat_axis=0, tiled=True)
    rope_full = lax.all_gather(rope_key[0], "sp", axis=0, tiled=True)
    grads_heads, rope_full_grad = attend_backward(arrived, rope_full)
    returned = lax.all_to_all(grads_heads, "sp", split_axis=0, concat_axis=1, tiled=True)
    rope_grad = lax.psum_scatter(rope_full_grad, "sp", scatter_dimension=0, tiled=True)
    query_grad = returned[:, :, :width].reshape(tokens, ATTENTION_HEADS * width)
    key_cols = returned[:, :, width : width + PLAIN_HEAD_WIDTH].reshape(tokens, head_cols)
    value_cols = returned[:, :, width + PLAIN_HEAD_WIDTH :].reshape(tokens, head_cols)
    dkv = jnp.stack([key_cols, value_cols], axis=1)
    d_nlat = jnp.einsum("tgn,gnc->tc", dkv, whole, preferred_element_type=f32)
    latents_all = lax.all_gather(nlat[None], "dp", axis=0, tiled=True)
    columns = lax.all_to_all(dkv[None], "dp", split_axis=3, concat_axis=0, tiled=True)
    partial_value = jnp.einsum("stgr,stc->grc", columns, latents_all, preferred_element_type=f32)
    weight_grads = lax.psum(partial_value, "sp")
    gain_grad = lax.psum(jnp.sum(d_nlat * normed, axis=0), ("sp", "dp"))
    scaled = d_nlat * latent_norm_gain
    latent_grad = inv_rms * (scaled - normed * jnp.mean(scaled * normed, axis=-1, keepdims=True))
    return (
        query_grad[None],
        latent_grad[None],
        rope_grad[None],
        weight_grads[0],
        weight_grads[1],
        gain_grad,
    )


def solution(mesh):
    in_specs = (
        P("dp", "sp", None),
        P("dp", "sp", None),
        P("dp", "sp", None),
        P(),
        P("dp", None),
        P("dp", None),
        P("dp", "sp", None),
    )
    out_specs = (
        P("dp", "sp", None),
        P("dp", "sp", None),
        P("dp", "sp", None),
        P("dp", None),
        P("dp", None),
        P(),
    )
    return jax.shard_map(local, mesh=mesh, in_specs=in_specs, out_specs=out_specs, check_vma=False)
```

profile of v0, /device:TPU:0, one launch (start us, length us, event | category | flops | bytes accessed | tf_op | source)
XLA Modules:
  0.0 738.0 jit_solution(6265751976223707838)
XLA Ops:
  7.2 3.1 pad_maximum_fusion.2
  12.3 3.9 reshape_squeeze.12
  16.4 55.1 %all-gather.4.cloned.1.call-done = bf16[2,2048,1024]{2,1,0:T(8,128)(2,1)} async-done(((bf16[2,512,1024]{2,1,0:T(8,128)(2,1)}), bf16[2,2048,1024]{2,1,0:T(8,128)(2,1)}) %all-gather.4.cloned.1.call-update) | async-done | bytes 8388624 | tf_op jit(solution)/shard_map/all_gather | solution.py:99
  71.5 6.2 convolution_convert_fusion
  84.6 3.1 copy.95
  87.8 5.6 pad_maximum_fusion
  93.4 4.0 copy.97
  97.4 5.6 all-to-all-start
  103.2 126.8 %all-gather = bf16[1,1536,32]{2,0,1:T(2,128)(2,1)S(1)} all-gather(bf16[1,192,32]{2,0,1:T(2,128)(2,1)S(1)} %copy.99), channel_id=2, replica_groups=mesh['sp'=8,'dp'=4] {'sp'}, dimensions={1}, use_global_device_ids=true | all-gather | bytes 110592 | tf_op jit(solution)/shard_map/all_gather | solution.py:107
  236.4 8.3 %copy.98 = bf16[8,192,4,288]{1,0,3,2:T(8,128)(2,1)} copy(bf16[8,192,4,288]{3,1,2,0:T(8,128)(2,1)} %bitcast.8) | data formatting | bytes 7077888 | tf_op jit(solution)/shard_map/all_to_all | solution.py:106
  244.7 6.9 all_to_all.42
  254.7 3.3 fusion.152
  258.0 5.4 fusion.43
  263.4 3.1 multiply_reduce_fusion.2
  274.4 3.2 fusion.6
  280.8 2.8 multiply_reduce_fusion.1
  283.7 9.7 %multiply_convert_fusion.1 = bf16[4,512,1024]{2,1,0:T(8,128)(2,1)S(1)} fusion(f32[4,512,1024]{2,1,0:T(8,128)S(1)} %get-tuple-element.177, f32[4,512]{1,0:T(4,128)S(1)} %get-tuple-element.176, f32[4,512,1024]{2,1,0:T(8,128)S(1)} %get-tuple-element.171, f32[4,512]{1,0:T(4,128)S(1)} %get-tuple-element.170), kind=kLoop, calls=%fused_computation.12 | loop fusion | flops 8388608 | bytes 20987904 | tf_op jit(solution)/shard_map/convert_element_type | solution.py:68
  295.5 3.1 fusion.50
  300.5 8.5 %fusion.4 = f32[4,512,1536]{2,1,0:T(8,128)} fusion(f32[1536,512,4]{0,1,2:T(8,128)S(1)} %fusion.114, pred[512,1536]{1,0:T(8,128)(4,1)S(1)} %copy-done.13, bf16[1536,4,288]{0,2,1:T(8,128)(2,1)} %copy-done.3), kind=kOutput, calls=%fused_computation.5 | convolution fusion | flops 412090368 | bytes 27000832 | tf_op jit(solution)/shard_map/qhd,khd->hqk/dot_general | solution.py:57
  309.1 14.9 %fusion.154 = (f32[4,512]{1,0:T(4,128)S(1)}, f32[4,512,1536]{2,1,0:T(8,128)}) fusion(f32[4,512,1536]{2,1,0:T(8,128)} %fusion.4), kind=kOutput, calls=%fused_computation.226 | output fusion | flops 6292991 | bytes 25174016 | tf_op jit(solution)/shard_map/sub | solution.py:65
  323.9 11.8 %multiply_reduce_fusion = (f32[4,512]{1,0:T(4,128)S(1)}, f32[4,512,1536]{2,1,0:T(8,128)}) fusion(f32[4,512,1536]{2,1,0:T(8,128)} %get-tuple-element.173, f32[4,512]{1,0:T(4,128)S(1)} %get-tuple-element.172, bf16[1536,4,288]{0,2,1:T(8,128)(2,1)} %copy-done.3), kind=kOutput, calls=%fused_computation.7 | convolution fusion | flops 412088320 | bytes 26230784 | tf_op jit(solution)/shard_map/qhd,khd->hqk/dot_general | solution.py:66
  335.7 6.0 multiply_convert_fusion
  341.8 4.5 fusion.52
  346.3 2.7 fusion.53
  351.6 11.2 %fusion.37 = f32[1536,4,64]{0,2,1:T(8,128)} fusion(f32[1536,4,64]{0,2,1:T(8,128)} %scatter-add.24, bf16[1536,4,288]{0,2,1:T(8,128)(2,1)} %copy-done.3, f32[4,512]{1,0:T(4,128)S(1)} %get-tuple-element.170, f32[4,512,1024]{2,1,0:T(8,128)} %copy-done.2), kind=kOutput, calls=%fused_computation.53 | convolution fusion | flops 274992128 | bytes 19144704 | tf_op jit(solution)/shard_map/hqk,qhd->khd/dot_general | solution.py:81
  362.8 4.4 fusion.42
  367.2 13.7 %fusion.22 = bf16[1536,4,64]{0,2,1:T(8,128)(2,1)} fusion(f32[1536,4,64]{0,2,1:T(8,128)} %fusion.37, bf16[1536,4,288]{0,2,1:T(8,128)(2,1)} %copy-done.3, f32[4,512]{1,0:T(4,128)S(1)} %get-tuple-element.172, f32[4,512,1536]{2,1,0:T(8,128)} %fusion.4), kind=kOutput, calls=%fused_computation.36 | convolution fusion | flops 412880384 | bytes 27795456 | tf_op jit(solution)/shard_map/hqk,qhd->khd/dot_general | solution.py:81
  381.0 4.6 fusion.21
  385.9 3.0 pad_maximum_fusion.1
  388.8 5.8 copy.107
  394.6 4.6 all-to-all-start.1
  401.9 64.4 %all-to-all-done.1 = bf16[1536,4,224]{2,1,0:T(4,128)(2,1)} async-done(((bf16[1536,4,224]{2,1,0:T(4,128)(2,1)}), bf16[1536,4,224]{2,1,0:T(4,128)(2,1)}, u32[]{:S(2)}, u32[]{:S(2)}) %all-to-all-start.1) | async-done | bytes 2752544 | tf_op jit(solution)/shard_map/all_to_all | solution.py:109
  468.8 2.8 fusion.149
  471.5 2.6 copy.111
  481.1 2.7 fusion.60
  483.8 6.1 copy.116
  489.8 4.4 all-to-all-start.2
  494.3 3.7 fusion.58
  498.0 4.0 fusion.26
  503.7 16.3 %all-to-all-done.2 = bf16[1,192,2,2048]{1,2,0,3:T(2,128)(2,1)} async-done(((bf16[1,192,2,2048]{1,2,0,3:T(2,128)(2,1)}), bf16[1,192,2,2048]{1,2,0,3:T(2,128)(2,1)}, u32[]{:S(2)}, u32[]{:S(2)}) %all-to-all-start.2) | async-done | bytes 1572896 | tf_op jit(solution)/shard_map/all_to_all | solution.py:117
  520.0 6.0 copy.118
  526.0 5.7 convolution_bitcast_fusion.1
  531.7 34.6 %reduce-scatter.4.cloned.1.call-done = f32[192,32]{1,0:T(8,128)} async-done(((f32[1536,32]{1,0:T(8,128)}), f32[192,32]{1,0:T(8,128)}) %reduce-scatter.4.cloned.1.call-update) | async-done | bytes 24592
  569.2 3.0 broadcast_in_dim_reshape.3
  572.2 6.3 fusion.72
  578.5 44.0 %psum.15 = f32[1024]{0:T(1024)} all-reduce(f32[1024]{0:T(1024)S(1)} %get-tuple-element.138), channel_id=1, replica_groups=mesh['sp'=8,'dp'=4] {'sp','dp'}, use_global_device_ids=true, to_apply=%region_14.15 | all-reduce | flops 1024 | bytes 8192 | tf_op jit(solution)/shard_map/psum | solution.py:120
  623.6 102.6 %all-reduce.5.cloned.1.call-done = f32[2,512,1024]{2,1,0:T(8,128)} async-done(((f32[2,512,1024]{2,1,0:T(8,128)}), f32[2,512,1024]{2,1,0:T(8,128)}) %all-reduce.5.cloned.1.call-update) | async-done | bytes 4194320 | tf_op jit(solution)/shard_map/psum | solution.py:119
  726.2 4.8 slice_bitcast_fusion
  (168 shorter events, 54.3 us)
Async XLA Ops:
  7.2 3.2 copy-start.32
  7.2 64.3 %all-gather.4.cloned.1.call-start = ((), (), s32[]{:S(2)}) async-start(), calls=%async_computation.4 | async-start | bytes 10485760 | tf_op jit(solution)/shard_map/all_gather | solution.py:99
  10.3 5.9 copy-start.10
  10.4 61.1 %copy-start.41 = (f32[1024]{0:T(1024)S(1)}, f32[1024]{0:T(1024)}, u32[]{:S(2)}) copy-start(f32[1024]{0:T(1024)} %param.34) | copy-start | bytes 12292
  16.4 55.1 %copy-start.44 = (f32[192]{0:T(256)}, f32[192]{0:T(256)S(1)}, u32[]{:S(2)}) copy-start(f32[192]{0:T(256)S(1)} %add_rsqrt_fusion) | copy-start | bytes 2308
  97.4 5.7 copy-start.43
  97.4 139.0 %all-to-all-start = ((bf16[192,32,288]{2,0,1:T(8,128)(2,1)}), bf16[192,32,288]{2,0,1:T(8,128)(2,1)}, u32[]{:S(2)}, u32[]{:S(2)}) async-start(bf16[192,32,288]{2,0,1:T(8,128)(2,1)} %copy.97), calls=%async_computation | async-start | bytes 9437184 | tf_op jit(solution)/shard_map/all_to_all | solution.py:106
  251.6 11.8 %copy-start.3 = (bf16[1536,4,288]{0,2,1:T(8,128)(2,1)}, bf16[1536,4,288]{0,2,1:T(8,128)(2,1)S(1)}, u32[]{:S(2)}) copy-start(bf16[1536,4,288]{0,2,1:T(8,128)(2,1)S(1)} %all_to_all.42) | copy-start | bytes 10616836
  251.6 2.0 copy-start.16
  251.6 2.0 copy-start.18
  251.6 2.0 copy-start.24
  254.7 3.3 copy-start.5
  263.4 3.4 copy-start.4
  268.0 5.0 copy-start.7
  268.0 5.0 copy-start.9
  277.6 3.3 copy-start.2
  293.4 5.2 copy-start.1
  298.7 1.8 copy-start.13
  323.9 11.8 %slice-start = ((s8[12582912]{0:T(1024)(128)(4,1)}), s8[4194304]{0:T(1024)(128)(4,1)S(1)}, s32[]{:S(2)}) async-start(s8[12582912]{0:T(1024)(128)(4,1)} %bitcast.187), calls=%async_computation.8 | async-start | bytes 8388608
  323.9 11.8 %slice-start.1 = ((s8[12582912]{0:T(1024)(128)(4,1)}), s8[4194304]{0:T(1024)(128)(4,1)S(1)}, s32[]{:S(2)}) async-start(s8[12582912]{0:T(1024)(128)(4,1)} %bitcast.187), calls=%async_computation.9 | async-start | bytes 8388608
  323.9 11.8 %slice-start.2 = ((s8[12582912]{0:T(1024)(128)(4,1)}), s8[4194304]{0:T(1024)(128)(4,1)S(1)}, s32[]{:S(2)}) async-start(s8[12582912]{0:T(1024)(128)(4,1)} %bitcast.187), calls=%async_computation.10 | async-start | bytes 8388608
  341.8 7.1 copy-start
  346.3 2.7 copy-start.34
  380.9 4.7 copy-start.21
  380.9 4.8 copy-start.39
  380.9 4.8 copy-start.40
  380.9 4.8 copy-start.22
  380.9 4.8 copy-start.37
  380.9 4.8 copy-start.38
  380.9 4.9 copy-start.23
  380.9 4.9 copy-start.35
  380.9 4.9 copy-start.36
  380.9 4.9 copy-start.25
  381.0 4.9 copy-start.26
  381.0 4.9 copy-start.27
  381.0 4.9 copy-start.33
  394.6 4.9 copy-start.11
  394.6 4.9 copy-start.42
  394.6 4.9 copy-start.45
  394.6 71.6 %all-to-all-start.1 = ((bf16[1536,4,224]{2,1,0:T(4,128)(2,1)}), bf16[1536,4,224]{2,1,0:T(4,128)(2,1)}, u32[]{:S(2)}, u32[]{:S(2)}) async-start(bf16[1536,4,224]{2,1,0:T(4,128)(2,1)} %copy.107), calls=%async_computation.1 | async-start | bytes 6291456 | tf_op jit(solution)/shard_map/all_to_all | solution.py:109
  399.2 126.8 %all-gather.6.cloned.1.call-start = ((), (), s32[]{:S(2)}) async-start(), calls=%async_computation.5 | async-start | bytes 1966080 | tf_op jit(solution)/shard_map/all_gather | solution.py:116
  489.8 30.2 %all-to-all-start.2 = ((bf16[1,192,2,2048]{1,2,0,3:T(2,128)(2,1)}), bf16[1,192,2,2048]{1,2,0,3:T(2,128)(2,1)}, u32[]{:S(2)}, u32[]{:S(2)}) async-start(bf16[1,192,2,2048]{1,2,0,3:T(2,128)(2,1)} %copy.116), calls=%async_computation.2 | async-start | bytes 4194304 | tf_op jit(solution)/shard_map/all_to_all | solution.py:117
  494.3 72.0 %reduce-scatter.4.cloned.1.call-start = ((), (), s32[]{:S(2)}) async-start(), calls=%async_computation.7 | async-start | bytes 884736
  498.0 4.0 copy-start.47
  503.6 222.6 %all-reduce.5.cloned.1.call-start = ((), (), s32[]{:S(2)}) async-start(), calls=%async_computation.6 | async-start | bytes 8388608 | tf_op jit(solution)/shard_map/psum | solution.py:119
  567.9 4.3 copy-start.12
  568.2 4.0 copy-start.14
  568.2 4.0 copy-start.15
  (10 other events, 9.7 us)
Sparse Core Ops, SparseCore 0:
  10.5 60.9 all-gather.3
  401.6 19.9 all-gather.5
  503.8 62.4 reduce-scatter.3
  569.8 156.3 all-reduce.4
where the time goes:
time: 747 us; the launch traced here: 738 us
  waiting for transfers between devices  273 us (37%)
  blocking collectives  171 us (23%)
  matrix products  118 us (16%)
  local copies, waits for them, and re-layouts  87 us (12%)
  other arithmetic  59.6 us (8%)
  starting transfers between devices  15.1 us (2%)
  between operations  15 us (2%)
    all_gather x1, blocking collectives, local(): rope_full = lax.all_gather(rope_key[0], 'sp', axis=0, tiled=True)  127 us
    psum x1, waiting for transfers between devices, local(): weight_grads = lax.psum(partial_value, 'sp')  103 us
    all_to_all x1, waiting for transfers between devices, local(): lax.all_to_all(grads_heads, 'sp', split_axis=0, concat_axis=1, tiled=True)  64.4 us
    all_gather x1, waiting for transfers between devices, local(): whole = lax.all_gather(stacked, 'dp', axis=1, tiled=True)  55.1 us
    psum x1, blocking collectives, local(): gain_grad = lax.psum(jnp.sum(d_nlat * normed, axis=0), ('sp', 'dp'))  44 us
    unnamed x5, waiting for transfers between devices  34.6 us
    dot_general x3, matrix products, attend_backward(): jnp.einsum('hqk,qhd->khd', p_b, go, preferred_element_type=f32)  30.3 us
    sub x3, other arithmetic, attend_backward(): probs = jax.nn.softmax(scores, axis=-1)  20.1 us
  transfers between devices with their start and end apart: 7, of which 5 were waited for; matrix products, arithmetic and copies ran while one was open for 10% of the time, Pallas kernels for 0%

commit v1 on v0

--- a/solution.py
+++ b/solution.py
@@ -10,6 +10,14 @@
 SPAN = 64
 eps = 1e-06
 rope_base = 10000.0
+
+
+def doubling_sum(block, mesh_axis):
+    size, total = (lax.axis_size(mesh_axis), block)
+    for far in [1 << k for k in range(size.bit_length() - 1)]:
+        pairs = [(i, i ^ far) for i in range(size)]
+        total = total + lax.ppermute(total, mesh_axis, pairs)
+    return total
 
 
 def rotate(values, cosine, sine):
@@ -116,7 +124,7 @@
     latents_all = lax.all_gather(nlat[None], "dp", axis=0, tiled=True)
     columns = lax.all_to_all(dkv[None], "dp", split_axis=3, concat_axis=0, tiled=True)
     partial_value = jnp.einsum("stgr,stc->grc", columns, latents_all, preferred_element_type=f32)
-    weight_grads = lax.psum(partial_value, "sp")
+    weight_grads = doubling_sum(partial_value, "sp")
     gain_grad = lax.psum(jnp.sum(d_nlat * normed, axis=0), ("sp", "dp"))
     scaled = d_nlat * latent_norm_gain
     latent_grad = inv_rms * (scaled - normed * jnp.mean(scaled * normed, axis=-1, keepdims=True))

time: 747 us -> 1000 us (1.34)
  waiting for transfers between devices: 273 us -> 519 us
  blocking collectives: 171 us -> 197 us
    ppermute x0 -> x3, waiting for transfers between devices: none -> 182 us  [doubling_sum(): total = total + lax.ppermute(total, mesh_axis, pairs)]
    unnamed x5 -> x4, waiting for transfers between devices: 34.6 us -> 216 us
    psum x1 -> x0, waiting for transfers between devices: 103 us -> none  [local(): weight_grads = lax.psum(partial_value, 'sp')]
    all_to_all x0 -> x1, blocking collectives: none -> 30.3 us  [local(): lax.all_to_all(dkv[None], 'dp', split_axis=3, concat_axis=0, tiled=True)]
    all_to_all x1 -> x0, waiting for transfers between devices: 16.3 us -> none  [local(): lax.all_to_all(dkv[None], 'dp', split_axis=3, concat_axis=0, tiled=True)]
  transfers between devices with their start and end apart: 7 -> 8, of which waited for: 5 -> 5; matrix products, arithmetic and copies ran while one was open for 10% -> 6% of each run, Pallas kernels for 0% -> 0%
where the time goes in v1:
time: 1000 us; the launch traced here: 994 us
  waiting for transfers between devices  519 us (52%)
  blocking collectives  197 us (20%)
  matrix products  109 us (11%)
  local copies, waits for them, and re-layouts  82 us (8%)
  other arithmetic  60.4 us (6%)
  between operations  15 us (2%)
  starting transfers between devices  11.7 us (1%)
    unnamed x4, waiting for transfers between devices  216 us
    ppermute x3, waiting for transfers between devices, doubling_sum(): total = total + lax.ppermute(total, mesh_axis, pairs)  182 us
    all_gather x1, blocking collectives, local(): rope_full = lax.all_gather(rope_key[0], 'sp', axis=0, tiled=True)  127 us
    all_to_all x1, waiting for transfers between devices, local(): lax.all_to_all(grads_heads, 'sp', split_axis=0, concat_axis=1, tiled=True)  66 us
    all_gather x1, waiting for transfers between devices, local(): whole = lax.all_gather(stacked, 'dp', axis=1, tiled=True)  55.1 us
    psum x1, blocking collectives, local(): gain_grad = lax.psum(jnp.sum(d_nlat * normed, axis=0), ('sp', 'dp'))  40 us
    all_to_all x1, blocking collectives, local(): lax.all_to_all(dkv[None], 'dp', split_axis=3, concat_axis=0, tiled=True)  30.3 us
    dot_general x3, matrix products, attend_backward(): jnp.einsum('hqk,qhd->khd', p_b, go, preferred_element_type=f32)  30.3 us
  transfers between devices with their start and end apart: 8, of which 5 were waited for; matrix products, arithmetic and copies ran while one was open for 6% of the time, Pallas kernels for 0%

profile of v1, /device:TPU:0, one launch (start us, length us, event | category | flops | bytes accessed | tf_op | source)
XLA Modules:
  0.0 993.9 jit_solution(9897075457730060516)
XLA Ops:
  7.2 3.1 pad_maximum_fusion.2
  12.3 3.9 reshape_squeeze.12
  16.4 55.1 %all-gather.4.cloned.1.call-done = bf16[2,2048,1024]{2,1,0:T(8,128)(2,1)} async-done(((bf16[2,512,1024]{2,1,0:T(8,128)(2,1)}), bf16[2,2048,1024]{2,1,0:T(8,128)(2,1)}) %all-gather.4.cloned.1.call-update) | async-done | bytes 8388624 | tf_op jit(solution)/shard_map/all_gather | solution.py:107
  71.5 6.2 convolution_convert_fusion
  80.0 2.4 copy.94
  84.6 3.1 copy.95
  87.8 5.6 pad_maximum_fusion
  93.4 4.0 copy.97
  97.4 5.6 all-to-all-start
  103.1 126.8 %all-gather = bf16[1,1536,32]{2,0,1:T(2,128)(2,1)S(1)} all-gather(bf16[1,192,32]{2,0,1:T(2,128)(2,1)S(1)} %copy.99), channel_id=2, replica_groups=mesh['sp'=8,'dp'=4] {'sp'}, dimensions={1}, use_global_device_ids=true | all-gather | bytes 110592 | tf_op jit(solution)/shard_map/all_gather | solution.py:115
  236.3 8.3 copy.98
  244.6 6.9 all_to_all.42
  254.6 3.3 fusion.152
  257.9 5.4 fusion.43
  263.3 3.1 multiply_reduce_fusion.2
  274.3 3.2 fusion.6
  280.8 2.8 multiply_reduce_fusion.1
  287.5 3.1 fusion.50
  292.5 8.6 fusion.4
  301.1 14.9 %fusion.154 = (f32[4,512]{1,0:T(4,128)S(1)}, f32[4,512,1536]{2,1,0:T(8,128)}) fusion(f32[4,512,1536]{2,1,0:T(8,128)} %fusion.4), kind=kOutput, calls=%fused_computation.226 | output fusion | flops 6292991 | bytes 25174016 | tf_op jit(solution)/shard_map/sub | solution.py:73
  316.0 11.8 %multiply_reduce_fusion = (f32[4,512]{1,0:T(4,128)S(1)}, f32[4,512,1536]{2,1,0:T(8,128)}) fusion(f32[4,512,1536]{2,1,0:T(8,128)} %get-tuple-element.173, f32[4,512]{1,0:T(4,128)S(1)} %get-tuple-element.172, bf16[1536,4,288]{0,2,1:T(8,128)(2,1)} %copy-done.4), kind=kOutput, calls=%fused_computation.7 | convolution fusion | flops 412088320 | bytes 26230784 | tf_op jit(solution)/shard_map/qhd,khd->hqk/dot_general | solution.py:74
  327.8 6.0 multiply_convert_fusion
  333.8 4.5 fusion.52
  338.3 2.6 fusion.53
  343.6 11.2 %fusion.37 = f32[1536,4,64]{0,2,1:T(8,128)} fusion(f32[1536,4,64]{0,2,1:T(8,128)} %scatter-add.24, bf16[1536,4,288]{0,2,1:T(8,128)(2,1)} %copy-done.4, f32[4,512]{1,0:T(4,128)S(1)} %get-tuple-element.170, f32[4,512,1024]{2,1,0:T(8,128)} %copy-done.3), kind=kOutput, calls=%fused_computation.53 | convolution fusion | flops 274992128 | bytes 19144704 | tf_op jit(solution)/shard_map/hqk,qhd->khd/dot_general | solution.py:89
  354.8 4.4 fusion.42
  359.2 13.7 %fusion.22 = bf16[1536,4,64]{0,2,1:T(8,128)(2,1)} fusion(f32[1536,4,64]{0,2,1:T(8,128)} %fusion.37, bf16[1536,4,288]{0,2,1:T(8,128)(2,1)} %copy-done.4, f32[4,512]{1,0:T(4,128)S(1)} %get-tuple-element.172, f32[4,512,1536]{2,1,0:T(8,128)} %fusion.4), kind=kOutput, calls=%fused_computation.36 | convolution fusion | flops 412880384 | bytes 27795456 | tf_op jit(solution)/shard_map/hqk,qhd->khd/dot_general | solution.py:89
  373.0 4.6 fusion.21
  377.9 3.0 pad_maximum_fusion.1
  380.9 5.8 copy.107
  386.7 4.6 all-to-all-start.1
  392.4 66.0 %all-to-all-done.1 = bf16[1536,4,224]{2,1,0:T(4,128)(2,1)} async-done(((bf16[1536,4,224]{2,1,0:T(4,128)(2,1)}), bf16[1536,4,224]{2,1,0:T(4,128)(2,1)}, u32[]{:S(2)}, u32[]{:S(2)}) %all-to-all-start.1) | async-done | bytes 2752544 | tf_op jit(solution)/shard_map/all_to_all | solution.py:117
  458.4 2.3 copy.108
  462.6 2.7 fusion.149
  471.5 2.7 fusion.60
  474.2 6.1 copy.116
  480.2 30.3 %all_to_all.54 = bf16[1,192,2,2048]{1,2,0,3:T(2,128)(2,1)} all-to-all(bf16[1,192,2,2048]{1,2,0,3:T(2,128)(2,1)} %copy.116), channel_id=1, replica_groups=mesh['sp'=8,'dp'=4] {'dp'}, dimensions={3} | all-to-all | bytes 3145728 | tf_op jit(solution)/shard_map/all_to_all | solution.py:125
  510.6 6.0 copy.118
  516.6 3.7 convolution_bitcast_fusion.1
  521.6 90.7 %collective-permute-done = f32[2,512,1024]{2,1,0:T(8,128)S(1)} collective-permute-done((f32[2,512,1024]{2,1,0:T(8,128)S(1)}, f32[2,512,1024]{2,1,0:T(8,128)S(1)}, u32[]{:S(2)}, u32[]{:S(2)}) %collective-permute-start) | collective-permute-done | bytes 4194336 | tf_op jit(solution)/shard_map/ppermute | solution.py:19
  613.8 91.1 %collective-permute-done.1 = f32[2,512,1024]{2,1,0:T(8,128)S(1)} collective-permute-done((f32[2,512,1024]{2,1,0:T(8,128)S(1)}, f32[2,512,1024]{2,1,0:T(8,128)S(1)}, u32[]{:S(2)}, u32[]{:S(2)}) %collective-permute-start.1) | collective-permute-done | bytes 4194336 | tf_op jit(solution)/shard_map/ppermute | solution.py:19
  704.9 2.9 add.194
  712.3 215.7 %reduce-scatter.4.cloned.1.call-done = f32[192,32]{1,0:T(8,128)} async-done(((f32[1536,32]{1,0:T(8,128)}), f32[192,32]{1,0:T(8,128)}) %reduce-scatter.4.cloned.1.call-update) | async-done | bytes 24592
  930.9 3.0 broadcast_in_dim_reshape.3
  933.9 5.3 fusion.72
  939.2 40.0 %psum.7 = f32[1024]{0:T(1024)} all-reduce(f32[1024]{0:T(1024)S(1)} %get-tuple-element.138), channel_id=1, replica_groups=mesh['sp'=8,'dp'=4] {'sp','dp'}, use_global_device_ids=true, to_apply=%region_13.14 | all-reduce | flops 1024 | bytes 8192 | tf_op jit(solution)/shard_map/psum | solution.py:128
  980.3 4.4 add.195
  984.7 2.3 slice_bitcast_fusion
  (184 shorter events, 56.1 us)
Async XLA Ops:
  7.2 3.2 copy-start.35
  7.2 64.3 %all-gather.4.cloned.1.call-start = ((), (), s32[]{:S(2)}) async-start(), calls=%async_computation.4 | async-start | bytes 10485760 | tf_op jit(solution)/shard_map/all_gather | solution.py:107
  10.3 5.9 copy-start.13
  10.4 61.1 %copy-start.44 = (f32[1024]{0:T(1024)S(1)}, f32[1024]{0:T(1024)}, u32[]{:S(2)}) copy-start(f32[1024]{0:T(1024)} %param.34) | copy-start | bytes 12292
  16.4 55.1 %copy-start.47 = (f32[192]{0:T(256)}, f32[192]{0:T(256)S(1)}, u32[]{:S(2)}) copy-start(f32[192]{0:T(256)S(1)} %add_rsqrt_fusion) | copy-start | bytes 2308
  97.4 5.7 copy-start.46
  97.4 139.0 %all-to-all-start = ((bf16[192,32,288]{2,0,1:T(8,128)(2,1)}), bf16[192,32,288]{2,0,1:T(8,128)(2,1)}, u32[]{:S(2)}, u32[]{:S(2)}) async-start(bf16[192,32,288]{2,0,1:T(8,128)(2,1)} %copy.97), calls=%async_computation | async-start | bytes 9437184 | tf_op jit(solution)/shard_map/all_to_all | solution.py:114
  251.5 11.8 %copy-start.4 = (bf16[1536,4,288]{0,2,1:T(8,128)(2,1)}, bf16[1536,4,288]{0,2,1:T(8,128)(2,1)S(1)}, u32[]{:S(2)}) copy-start(bf16[1536,4,288]{0,2,1:T(8,128)(2,1)S(1)} %all_to_all.42) | copy-start | bytes 10616836
  254.5 3.3 copy-start.8
  263.3 3.4 copy-start.7
  267.9 5.0 copy-start.10
  267.9 5.0 copy-start.12
  277.5 3.3 copy-start.3
  285.5 5.2 copy-start.1
  316.0 11.8 %slice-start.2 = ((s8[12582912]{0:T(1024)(128)(4,1)}), s8[4194304]{0:T(1024)(128)(4,1)S(1)}, s32[]{:S(2)}) async-start(s8[12582912]{0:T(1024)(128)(4,1)} %bitcast.189), calls=%async_computation.9 | async-start | bytes 8388608
  316.0 11.8 %slice-start.3 = ((s8[12582912]{0:T(1024)(128)(4,1)}), s8[4194304]{0:T(1024)(128)(4,1)S(1)}, s32[]{:S(2)}) async-start(s8[12582912]{0:T(1024)(128)(4,1)} %bitcast.189), calls=%async_computation.10 | async-start | bytes 8388608
  316.0 11.8 %slice-start.4 = ((s8[12582912]{0:T(1024)(128)(4,1)}), s8[4194304]{0:T(1024)(128)(4,1)S(1)}, s32[]{:S(2)}) async-start(s8[12582912]{0:T(1024)(128)(4,1)} %bitcast.189), calls=%async_computation.11 | async-start | bytes 8388608
  333.8 7.1 copy-start
  338.3 2.7 copy-start.37
  372.9 4.7 copy-start.24
  372.9 4.8 copy-start.42
  372.9 4.8 copy-start.43
  372.9 4.8 copy-start.25
  372.9 4.8 copy-start.40
  372.9 4.8 copy-start.41
  372.9 4.9 copy-start.26
  373.0 4.9 copy-start.38
  373.0 4.9 copy-start.39
  373.0 4.9 copy-start.28
  373.0 4.9 copy-start.29
  373.0 4.9 copy-start.30
  373.0 4.9 copy-start.36
  386.7 4.6 copy-start.14
  386.7 4.7 copy-start.45
  386.7 4.7 copy-start.48
  386.7 71.7 %all-to-all-start.1 = ((bf16[1536,4,224]{2,1,0:T(4,128)(2,1)}), bf16[1536,4,224]{2,1,0:T(4,128)(2,1)}, u32[]{:S(2)}, u32[]{:S(2)}) async-start(bf16[1536,4,224]{2,1,0:T(4,128)(2,1)} %copy.107), calls=%async_computation.1 | async-start | bytes 6291456 | tf_op jit(solution)/shard_map/all_to_all | solution.py:117
  391.3 125.3 %all-gather.6.cloned.1.call-start = ((), (), s32[]{:S(2)}) async-start(), calls=%async_computation.5 | async-start | bytes 1966080 | tf_op jit(solution)/shard_map/all_gather | solution.py:124
  392.3 535.7 %reduce-scatter.4.cloned.1.call-start = ((), (), s32[]{:S(2)}) async-start(), calls=%async_computation.6 | async-start | bytes 884736
  520.3 92.0 %collective-permute-start = (f32[2,512,1024]{2,1,0:T(8,128)S(1)}, f32[2,512,1024]{2,1,0:T(8,128)S(1)}, u32[]{:S(2)}, u32[]{:S(2)}) collective-permute-start(f32[2,512,1024]{2,1,0:T(8,128)S(1)} %convolution_bitcast_fusion.1), channel_id=1, source_target_pairs={{0,4},{4,0},{8,12},{12,8},{16,20},{20,16},{24,28},{28,24},{1,5},{5... | collective-permute-start | bytes 12582920 | tf_op jit(solution)/shard_map/ppermute | solution.py:19
  612.3 97.1 %slice-start = ((s8[6291456]{0:T(1024)(128)(4,1)}), s8[4194304]{0:T(1024)(128)(4,1)S(1)}, s32[]{:S(2)}) async-start(s8[6291456]{0:T(1024)(128)(4,1)} %bitcast.187), calls=%async_computation.7 | async-start | bytes 8388608
  613.7 94.8 %copy-start.2 = (bf16[4,512,1024]{2,1,0:T(8,128)(2,1)S(1)}, bf16[4,512,1024]{2,1,0:T(8,128)(2,1)}, u32[]{:S(2)}) copy-start(bf16[4,512,1024]{2,1,0:T(8,128)(2,1)} %copy-done.1) | copy-start | bytes 12582916
  613.7 95.7 %slice-start.1 = ((s8[6291456]{0:T(1024)(128)(4,1)}), s8[2097152]{0:T(1024)(128)(4,1)S(1)}, s32[]{:S(2)}) async-start(s8[6291456]{0:T(1024)(128)(4,1)} %bitcast.187), calls=%async_computation.8 | async-start | bytes 4194304
  613.7 91.2 %collective-permute-start.1 = (f32[2,512,1024]{2,1,0:T(8,128)S(1)}, f32[2,512,1024]{2,1,0:T(8,128)S(1)}, u32[]{:S(2)}, u32[]{:S(2)}) collective-permute-start(f32[2,512,1024]{2,1,0:T(8,128)S(1)} %add.193), channel_id=1, source_target_pairs={{0,8},{4,12},{8,0},{12,4},{16,24},{20,28},{24,16},{28,20},{1,9},{5... | collective-permute-start | bytes 12582920 | tf_op jit(solution)/shard_map/ppermute | solution.py:19
  707.8 272.5 %collective-permute-start.2 = (f32[2,512,1024]{2,1,0:T(8,128)}, f32[2,512,1024]{2,1,0:T(8,128)}, u32[]{:S(2)}, u32[]{:S(2)}) collective-permute-start(f32[2,512,1024]{2,1,0:T(8,128)} %add.194), channel_id=1, source_target_pairs={{0,16},{4,20},{8,24},{12,28},{16,0},{20,4},{24,8},{28,12},{1,17},{... | collective-permute-start | bytes 12582920 | tf_op jit(solution)/shard_map/ppermute | solution.py:19
  709.4 220.1 %copy-start.6 = (bf16[192,8,4,224]{3,0,2,1:T(8,128)(2,1)S(1)}, bf16[192,8,4,224]{3,0,2,1:T(8,128)(2,1)}, u32[]{:S(2)}) copy-start(bf16[192,8,4,224]{3,0,2,1:T(8,128)(2,1)} %copy-done.5) | copy-start | bytes 8257540
  929.6 4.3 copy-start.15
  929.9 4.0 copy-start.17
  929.9 4.0 copy-start.18
  (16 other events, 20.3 us)
Sparse Core Ops, SparseCore 0:
  10.5 60.9 all-gather.3
  394.3 19.9 all-gather.5
  712.4 215.5 reduce-scatter.3
